TPU v7x, 32 devices: a whole 2x2x4 slice. The times are simulated.
32 devices in a mesh: sp: 8 (over z, core), tp: 4 (over y, x).
Axes of the slice: x: 2, y: 2, z: 4, core: 2. Of those that a mesh axis runs over, the one named last changes fastest.
Arguments:
- residual: bfloat16 [896, 2048], P('sp'), may hold values from -1.5 to 1.5
- latent: bfloat16 [896, 512], P('sp'), may hold values from -6 to 6
- rot_key: bfloat16 [896, 64], P('sp'), may hold values from -6 to 6
- latent_norm_scale: float32 [512], replicated, may hold values from 0.1 to 1.9
- query_wide: bfloat16 [896, 3072], P('sp', 'tp'), may hold values from -210 to 210
- query_narrow: bfloat16 [896, 2048], P('sp', 'tp'), may hold values from -210 to 210
- large_key_lift: bfloat16 [512, 2048], P(None, 'tp'), may hold values from -0.25 to 0.25
- large_value_lift: bfloat16 [512, 2048], P(None, 'tp'), may hold values from -0.25 to 0.25
- small_key_lift: bfloat16 [512, 1024], P(None, 'tp'), may hold values from -0.25 to 0.25
- small_value_lift: bfloat16 [512, 1024], P(None, 'tp'), may hold values from -0.25 to 0.25
- out_wide: bfloat16 [2048, 2048], P('tp'), may hold values from -0.5 to 0.5
- out_narrow: bfloat16 [1024, 2048], P('tp'), may hold values from -0.75 to 0.75
- mix_gain: float32 [2048], replicated, may hold values from 0.1 to 1.9
- router_group: bfloat16 [2048, 4], replicated, may hold values from -0.125 to 0.125
- router_expert: bfloat16 [2048, 8], replicated, may hold values from -0.125 to 0.125
- expert_ids: int32 [896, 2], P('sp'), may hold values from 0 to 7, all different within a row; in each aligned block of 112 rows (0 to 111, 112 to 223, ...) at most 56 rows name the same one
- expert_gate_w: bfloat16 [8, 2048, 4096], P('sp', None, 'tp'), may hold values from -0.125 to 0.125
- expert_up_w: bfloat16 [8, 2048, 4096], P('sp', None, 'tp'), may hold values from -0.125 to 0.125
- expert_down_w: bfloat16 [8, 4096, 2048], P('sp', 'tp'), may hold values from -0.375 to 0.375
Outputs:
- updated: bfloat16 [896, 2048], P('sp', 'tp')
Inputs may be any that keep to these rules, and one draw needn't show every extreme that they name: `expert_ids`: each row names two different experts; the rows of one index of sp name no expert more than 56 times, a bound that some expert reaches in some of these blocks.
All inputs are finite; a program needn't handle non-finite values.
Results may differ from a plain program's by a relative error of at most 0.024.
The roundings to bfloat16 on the way count: a program that leaves them out, or rounds other values in their place, can miss the bound.
Values may be sent and summed in bfloat16 or wider, within the bound.
A program may use at most 64 MiB of HBM per device.

v0:
```python
import jax
import jax.numpy as jnp
from jax import lax
from jax.sharding import PartitionSpec as P

PLAIN_KEY_WIDTH = 128
LARGE_VALUE_SIZE = 128
SMALL_HEAD_WIDTH = 64
ROPE = 64
rope_base = 10000.0
epsilon = 1e-06
very_low = -1e30


def angle_table(positions, width):
    frequency = rope_base ** (-jnp.arange(0, width, 2, dtype=jnp.float32) / width)
    return positions.astype(jnp.float32)[:, None] * frequency[None, :]


def rotate(values, angles):
    half_width = values.shape[-1] // 2
    cosine = jnp.cos(angles)
    sine_part = jnp.sin(angles)
    front_half = values[..., :half_width]
    back_half = values[..., half_width:]
    return jnp.concatenate(
        [front_half * cosine - back_half * sine_part, front_half * sine_part + back_half * cosine],
        axis=-1,
    )


def rms_scale(values, gain):
    return values * lax.rsqrt(jnp.mean(values * values, axis=-1, keepdims=True) + epsilon) * gain


def roped_queries(query, plain_width, angles):
    row_count = query.shape[0]
    shaped = query.reshape(row_count, -1, plain_width + ROPE)
    turned = rotate(shaped[..., plain_width:].astype(jnp.float32), angles[:, None, :]).astype(
        jnp.bfloat16
    )
    return jnp.concatenate([shaped[..., :plain_width], turned], axis=-1)


def expand_keys(latent_rows, large_key_lift, large_value_lift, small_key_lift, small_value_lift):
    row_count = latent_rows.shape[0]

    def project(weight, head_width):
        product = jnp.dot(latent_rows, weight, preferred_element_type=jnp.float32).astype(
            jnp.bfloat16
        )
        return product.reshape(row_count, weight.shape[1] // head_width, head_width)

    return (
        project(large_key_lift, PLAIN_KEY_WIDTH),
        project(large_value_lift, LARGE_VALUE_SIZE),
        project(small_key_lift, SMALL_HEAD_WIDTH),
        project(small_value_lift, SMALL_HEAD_WIDTH),
    )


def attend_group(state, queries, plain_width, key_rows, values, key_rot, causal_mask):
    row_peak, weight_sum, summed = state
    score_scale = (plain_width + ROPE) ** (-0.5)
    scores = jnp.einsum(
        "qhd,khd->qhk", queries[..., :plain_width], key_rows, preferred_element_type=jnp.float32
    )
    scores = scores + jnp.einsum(
        "qhd,kd->qhk", queries[..., plain_width:], key_rot, preferred_element_type=jnp.float32
    )
    scores = scores * score_scale
    allowed = causal_mask[:, None, :]
    new_peak = jnp.maximum(row_peak, jnp.max(jnp.where(allowed, scores, very_low), axis=-1))
    weights = jnp.where(allowed, jnp.exp(scores - new_peak[..., None]), 0.0)
    weight_sum = jnp.sum(weights, axis=-1)
    summed = jnp.einsum(
        "qhk,khd->qhd", weights.astype(jnp.bfloat16), values, preferred_element_type=jnp.float32
    )
    return (new_peak, weight_sum, summed)


def shards(
    residual,
    latent,
    rot_key,
    latent_norm_scale,
    query_wide,
    query_narrow,
    large_key_lift,
    large_value_lift,
    small_key_lift,
    small_value_lift,
    out_wide,
    out_narrow,
    mix_gain,
    router_group,
    router_expert,
    expert_ids,
    expert_gate_w,
    expert_up_w,
    expert_down_w,
):
    tok_rows = latent.shape[0]
    positions = lax.axis_index("sp") * tok_rows + jnp.arange(tok_rows, dtype=jnp.int32)
    angles = angle_table(positions, ROPE)
    normed = rms_scale(latent.astype(jnp.float32), latent_norm_scale).astype(jnp.bfloat16)
    key_turned = rotate(rot_key.astype(jnp.float32), angles).astype(jnp.bfloat16)
    wide_queries = roped_queries(query_wide, PLAIN_KEY_WIDTH, angles)
    narrow_queries = roped_queries(query_narrow, SMALL_HEAD_WIDTH, angles)

    def empty_state(head_count, head_width):
        return (
            jnp.full((tok_rows, head_count), very_low, jnp.float32),
            jnp.zeros((tok_rows, head_count), jnp.float32),
            jnp.zeros((tok_rows, head_count, head_width), jnp.float32),
        )

    initial = (
        empty_state(wide_queries.shape[1], LARGE_VALUE_SIZE),
        empty_state(narrow_queries.shape[1], SMALL_HEAD_WIDTH),
    )
    key_set = expand_keys(
        lax.all_gather(normed, "sp", axis=0, tiled=True),
        large_key_lift,
        large_value_lift,
        small_key_lift,
        small_value_lift,
    )
    key_rot = lax.all_gather(key_turned, "sp", axis=0, tiled=True)
    key_positions = jnp.arange(key_rot.shape[0], dtype=jnp.int32)
    causal_mask = positions[:, None] >= key_positions[None, :]
    wide_state = attend_group(
        initial[0], wide_queries, PLAIN_KEY_WIDTH, key_set[0], key_set[1], key_rot, causal_mask
    )
    narrow_state = attend_group(
        initial[1], narrow_queries, SMALL_HEAD_WIDTH, key_set[2], key_set[3], key_rot, causal_mask
    )

    def heads_out(state):
        return (state[2] / state[1][..., None]).astype(jnp.bfloat16).reshape(tok_rows, -1)

    partial_value = jnp.dot(heads_out(wide_state), out_wide, preferred_element_type=jnp.float32)
    partial_value = partial_value + jnp.dot(
        heads_out(narrow_state), out_narrow, preferred_element_type=jnp.float32
    )
    rounded_partial = lax.optimization_barrier(partial_value.astype(jnp.bfloat16)).astype(
        jnp.float32
    )
    attended = lax.psum(rounded_partial.astype(jnp.bfloat16), "tp").astype(jnp.float32)
    mixed = residual.astype(jnp.float32) + attended
    normal_rows = rms_scale(mixed, mix_gain).astype(jnp.bfloat16)
    group_count = router_group.shape[1]
    expert_count = router_expert.shape[1]
    group_prob = jax.nn.softmax(
        jnp.dot(normal_rows, router_group, preferred_element_type=jnp.float32), axis=-1
    )
    logits = jnp.dot(normal_rows, router_expert, preferred_element_type=jnp.float32)
    chosen_group = expert_ids[:, 0] // (expert_count // group_count)
    group_pick = jnp.sum(
        jnp.where(chosen_group[:, None] == jnp.arange(group_count)[None, :], group_prob, 0.0),
        axis=1,
    )
    expert_match = expert_ids[:, :, None] == jnp.arange(expert_count)[None, None, :]
    chosen_logits = jnp.sum(jnp.where(expert_match, logits[:, None, :], 0.0), axis=2)
    gates = group_pick[:, None] * jax.nn.softmax(chosen_logits, axis=-1)
    tp_size = lax.axis_size("tp")
    sp_size = lax.axis_size("sp")
    capacity = tp_size * max(1, 4 * tok_rows // (expert_count * tp_size))
    flat_ids = expert_ids.reshape(-1)
    one_hot = (flat_ids[:, None] == jnp.arange(expert_count)[None, :]).astype(jnp.int32)
    earlier = jnp.cumsum(one_hot, axis=0) - one_hot
    slot_index = jnp.sum(earlier * one_hot, axis=1)
    target = flat_ids * capacity + slot_index
    source_row = jnp.arange(flat_ids.shape[0], dtype=jnp.int32) // 2
    row_of_slot = jnp.zeros((expert_count * capacity,), jnp.int32).at[target].set(source_row)
    slot_used = jnp.zeros((expert_count * capacity,), jnp.bool_).at[target].set(True)
    outgoing = jnp.where(slot_used[:, None], normal_rows[row_of_slot], jnp.zeros((), jnp.bfloat16))
    outgoing = outgoing.reshape(expert_count, capacity, -1)
    expert_rows = lax.all_to_all(outgoing, "sp", split_axis=0, concat_axis=1, tiled=True)
    lead_blocks = 1
    gate_part = jnp.einsum(
        "erd,edf->erf", expert_rows, expert_gate_w, preferred_element_type=jnp.float32
    )
    up_part = jnp.einsum(
        "erd,edf->erf", expert_rows, expert_up_w, preferred_element_type=jnp.float32
    )
    hidden = (jax.nn.silu(gate_part) * up_part).astype(jnp.bfloat16)
    down_part = jnp.einsum(
        "erf,efd->erd", hidden, expert_down_w, preferred_element_type=jnp.float32
    )
    rounded_down = lax.optimization_barrier(down_part.astype(jnp.bfloat16)).astype(jnp.float32)
    expert_out = lax.psum_scatter(
        rounded_down.astype(jnp.bfloat16), "tp", scatter_dimension=2, tiled=True
    )
    column_count = expert_out.shape[2]
    shaped_out = expert_out.reshape(expert_out.shape[0], lead_blocks, sp_size, -1, column_count)
    returned = lax.all_to_all(shaped_out, "sp", split_axis=2, concat_axis=0, tiled=True)
    returned = returned.reshape(expert_count * capacity, column_count)
    picked = returned[target].astype(jnp.float32).reshape(tok_rows, 2, column_count)
    combined = jnp.sum(picked * gates[:, :, None], axis=1)
    own_columns = lax.dynamic_slice_in_dim(
        mixed, lax.axis_index("tp") * column_count, column_count, 1
    )
    return (own_columns + combined).astype(jnp.bfloat16)


def solution(mesh):
    placed = (
        P("sp", None),
        P("sp", None),
        P("sp", None),
        P(),
        P("sp", "tp"),
        P("sp", "tp"),
        P(None, "tp"),
        P(None, "tp"),
        P(None, "tp"),
        P(None, "tp"),
        P("tp", None),
        P("tp", None),
        P(),
        P(),
        P(),
        P("sp", None),
        P("sp", None, "tp"),
        P("sp", None, "tp"),
        P("sp", "tp", None),
    )
    return jax.shard_map(
        shards, mesh=mesh, in_specs=placed, out_specs=P("sp", "tp"), check_vma=False
    )
```

profile of v0, /device:TPU:0, one launch (start us, length us, event | category | flops | bytes accessed | tf_op | source)
XLA Modules:
  0.0 230.2 jit_solution(13567661316674832507)
XLA Ops:
  6.6 0.9 convert_element_type.96
  7.5 1.1 copy.55
  8.6 1.0 copy.69
  9.6 0.1 multiply_cosine_fusion
  9.8 15.7 %all-gather = bf16[8,112,64]{1,2,0:T(8,128)(2,1)S(1)} all-gather(bf16[1,112,64]{1,2,0:T(8,128)(2,1)S(1)} %maximum_bitcast_fusion), channel_id=1, replica_groups=mesh['sp'=8,'tp'=4] {'sp'}, dimensions={0}, use_global_device_ids=true | all-gather | bytes 129024 | tf_op jit(solution)/shard_map/all_gather | solution.py:129
  25.6 0.1 reshape.332
  25.7 1.0 fusion.36
  26.8 1.0 fusion.38
  27.8 16.2 %all_gather.6 = bf16[896,512]{1,0:T(8,128)(2,1)S(1)} all-gather(bf16[112,512]{1,0:T(8,128)(2,1)S(1)} %fusion.38), channel_id=1, replica_groups=mesh['sp'=8,'tp'=4] {'sp'}, dimensions={0}, use_global_device_ids=true | all-gather | bytes 1032192 | tf_op jit(solution)/shard_map/all_gather | solution.py:123
  44.0 0.8 convolution_convert_fusion
  44.8 0.4 fusion.39
  45.4 0.4 copy-done.5
  45.7 0.5 convolution_convert_fusion.2
  46.2 0.4 fusion.44
  46.7 0.4 fusion.14
  47.1 0.9 select_reduce_fusion
  48.1 0.5 convolution_convert_fusion.3
  48.6 0.8 convolution_convert_fusion.1
  49.3 0.8 fusion.19
  50.2 0.5 fusion.25
  50.7 0.6 fusion.24
  51.3 0.5 fusion.41
  51.8 0.7 copy-done.4
  52.5 1.1 fusion.12
  53.8 0.1 eq.50
  54.0 0.6 reduce-window.6
  54.6 0.2 slice_reduce_fusion
  55.2 1.3 scatter_custom_fusion.1
  56.5 1.4 scatter_custom_fusion
  58.0 42.1 %all-reduce.3.cloned.1.call-done = bf16[112,2048]{1,0:T(8,128)(2,1)} async-done(((bf16[112,2048]{1,0:T(8,128)(2,1)}), bf16[112,2048]{1,0:T(8,128)(2,1)}) %all-reduce.3.cloned.1.call-update) | async-done | bytes 458768 | tf_op jit(solution)/shard_map/psum | solution.py:149
  100.2 2.3 convert_add_fusion
  102.5 0.2 multiply_convert_fusion.1
  102.7 3.2 %gather_fusion = bf16[448,2048]{1,0:T(8,128)(2,1)} fusion(bf16[112,2048]{1,0:T(8,128)(2,1)S(1)} %multiply_convert_fusion.1, s32[1024]{0:T(1024)S(1)} %pad_clamp_fusion.1), kind=kCustom, calls=%fused_computation | custom fusion | bytes 3671808 | tf_op jit(solution)/shard_map/gather | solution.py:177
  105.9 1.8 broadcast_select_fusion
  107.8 47.8 %all_to_all.8 = bf16[8,56,2048]{2,1,0:T(8,128)(2,1)S(1)} all-to-all(bf16[8,56,2048]{2,1,0:T(8,128)(2,1)S(1)} %broadcast_select_fusion), channel_id=1, replica_groups=mesh['sp'=8,'tp'=4] {'sp'}, dimensions={0} | all-to-all | bytes 3670016 | tf_op jit(solution)/shard_map/all_to_all | solution.py:179
  155.6 1.3 copy-done.1
  156.8 3.3 %fusion.4 = f32[448,1024]{1,0:T(8,128)} fusion(bf16[448,2048]{1,0:T(8,128)(2,1)S(1)} %bitcast.98, bf16[1,2048,1024]{2,1,0:T(8,128)(2,1)S(1)} %copy-done.11), kind=kOutput, calls=%fused_computation.8 | convolution fusion | flops 1879048192 | bytes 7864320 | tf_op jit(solution)/shard_map/erd,edf->erf/dot_general | solution.py:181
  160.2 9.8 %fusion.9 = bf16[1,448,2048]{2,1,0:T(8,128)(2,1)} fusion(bf16[1,1024,2048]{2,1,0:T(8,128)(2,1)} %param.37, f32[448,1024]{1,0:T(8,128)} %fusion.4, bf16[448,2048]{1,0:T(8,128)(2,1)} %bitcast.99, bf16[1,2048,1024]{2,1,0:T(8,128)(2,1)} %param.36), kind=kOutput, calls=%fused_computation.11 | convolution fusion | flops 3761766400 | bytes 13893632 | tf_op jit(solution)/shard_map/erf,efd->erd/dot_general | solution.py:188
  170.1 0.7 copy-done.7
  170.8 0.2 fusion.69
  171.0 30.2 %reduce-scatter.2.cloned.1.call-done = bf16[1,448,512]{2,1,0:T(8,128)(2,1)} async-done(((bf16[1,448,2048]{2,1,0:T(8,128)(2,1)}), bf16[1,448,512]{2,1,0:T(8,128)(2,1)}) %reduce-scatter.2.cloned.1.call-update) | async-done | bytes 458768 | tf_op jit(solution)/shard_map/reduce_scatter | solution.py:192
  201.2 4.6 %all-to-all-start.1 = ((bf16[1,1,8,56,512]{4,3,1,0,2:T(8,128)(2,1)}), bf16[1,1,8,56,512]{4,3,1,0,2:T(8,128)(2,1)S(1)}, u32[]{:S(2)}, u32[]{:S(2)}) async-start(bf16[1,1,8,56,512]{4,3,1,0,2:T(8,128)(2,1)} %bitcast.106), calls=%async_computation.2 | async-start | bytes 917504 | tf_op jit(solution)/shard_map/all_to_all | solution.py:197
  205.8 0.2 fusion.68
  206.3 13.4 %all-to-all-done.1 = bf16[1,1,8,56,512]{4,3,1,0,2:T(8,128)(2,1)S(1)} async-done(((bf16[1,1,8,56,512]{4,3,1,0,2:T(8,128)(2,1)}), bf16[1,1,8,56,512]{4,3,1,0,2:T(8,128)(2,1)S(1)}, u32[]{:S(2)}, u32[]{:S(2)}) %all-to-all-start.1) | async-done | bytes 458784 | tf_op jit(solution)/shard_map/all_to_all | solution.py:197
  219.7 1.1 gather_fusion.1
  220.8 0.3 reshape.296
  221.1 0.6 multiply_reduce_fusion.1
  221.7 1.6 add_convert_fusion
  (65 shorter events, 1.4 us)
Async XLA Ops:
  6.5 44.7 %copy-start = (bf16[512,2048]{1,0:T(8,128)(2,1)S(1)}, bf16[512,2048]{1,0:T(8,128)(2,1)}, u32[]{:S(2)}) copy-start(bf16[512,2048]{1,0:T(8,128)(2,1)} %param.29) | copy-start | bytes 6291460
  6.5 37.5 %copy-start.12 = (bf16[512,512]{1,0:T(8,128)(2,1)S(1)}, bf16[512,512]{1,0:T(8,128)(2,1)}, u32[]{:S(2)}) copy-start(bf16[512,512]{1,0:T(8,128)(2,1)} %param.25) | copy-start | bytes 1572868
  6.5 93.6 %all-reduce.3.cloned.1.call-start = ((), (), s32[]{:S(2)}) async-start(), calls=%async_computation.3 | async-start | bytes 917504 | tf_op jit(solution)/shard_map/psum | solution.py:149
  44.8 1.0 copy-start.5
  47.1 1.0 copy-start.6
  47.1 1.4 copy-start.13
  51.3 1.2 copy-start.4
  51.8 1.9 copy-start.9
  51.8 48.4 %copy-start.2 = (bf16[112,2048]{1,0:T(8,128)(2,1)S(1)}, bf16[112,2048]{1,0:T(8,128)(2,1)}, u32[]{:S(2)}) copy-start(bf16[112,2048]{1,0:T(8,128)(2,1)} %param.19) | copy-start | bytes 1376260
  53.6 48.8 %copy-start.10 = (f32[2048]{0:T(1024)S(1)}, f32[2048]{0:T(1024)}, u32[]{:S(2)}) copy-start(f32[2048]{0:T(1024)} %param.31) | copy-start | bytes 24580
  53.7 147.5 %reduce-scatter.2.cloned.1.call-start = ((), (), s32[]{:S(2)}) async-start(), calls=%async_computation.4 | async-start | bytes 2293760 | tf_op jit(solution)/shard_map/reduce_scatter | solution.py:192
  100.2 2.3 %copy-start.3 = (bf16[112,2048]{1,0:T(8,128)(2,1)S(1)}, bf16[112,2048]{1,0:T(8,128)(2,1)}, u32[]{:S(2)}) copy-start(bf16[112,2048]{1,0:T(8,128)(2,1)} %all-reduce.3.cloned.1.call-done) | copy-start | bytes 1376260
  105.9 50.9 %copy-start.11 = (bf16[1,2048,1024]{2,1,0:T(8,128)(2,1)S(1)}, bf16[1,2048,1024]{2,1,0:T(8,128)(2,1)}, u32[]{:S(2)}) copy-start(bf16[1,2048,1024]{2,1,0:T(8,128)(2,1)} %param.35) | copy-start | bytes 12582916
  155.6 1.3 copy-start.1
  170.0 0.8 copy-start.7
  170.0 35.8 %copy-start.8 = (bf16[2048,4]{0,1:T(4,128)(2,1)S(1)}, bf16[2048,4]{0,1:T(4,128)(2,1)}, u32[]{:S(2)}) copy-start(bf16[2048,4]{0,1:T(4,128)(2,1)} %param.32) | copy-start | bytes 49156
  201.2 18.5 %all-to-all-start.1 = ((bf16[1,1,8,56,512]{4,3,1,0,2:T(8,128)(2,1)}), bf16[1,1,8,56,512]{4,3,1,0,2:T(8,128)(2,1)S(1)}, u32[]{:S(2)}, u32[]{:S(2)}) async-start(bf16[1,1,8,56,512]{4,3,1,0,2:T(8,128)(2,1)} %bitcast.106), calls=%async_computation.2 | async-start | bytes 917504 | tf_op jit(solution)/shard_map/all_to_all | solution.py:197
Sparse Core Ops, SparseCore 0:
  53.8 46.3 all-reduce.2
  170.2 30.9 reduce-scatter.1
where the time goes:
time: 231 us; the launch traced here: 230 us
  waiting for transfers between devices  85.8 us (37%)
  blocking collectives  79.8 us (35%)
  matrix products  20.9 us (9%)
  between operations  13.8 us (6%)
  local copies, waits for them, and re-layouts  13.7 us (6%)
  other arithmetic  11.6 us (5%)
  starting transfers between devices  4.66 us (2%)
    all_to_all x1, blocking collectives, shards(): lax.all_to_all(outgoing, 'sp', split_axis=0, concat_axis=1, tiled=True)  47.8 us
    psum x1, waiting for transfers between devices, shards(): lax.psum(rounded_partial.astype(jnp.bfloat16), 'tp').astype(jnp.float32)  42.1 us
    reduce_scatter x1, waiting for transfers between devices, shards(): lax.psum_scatter(rounded_down.astype(jnp.bfloat16), 'tp', scatter_dimensi...  30.2 us
    all_gather x1, blocking collectives, shards(): lax.all_gather(normed, 'sp', axis=0, tiled=True)  16.2 us
    all_gather x1, blocking collectives, shards(): key_rot = lax.all_gather(key_turned, 'sp', axis=0, tiled=True)  15.7 us
    all_to_all x1, waiting for transfers between devices, shards(): lax.all_to_all(shaped_out, 'sp', split_axis=2, concat_axis=0, tiled=True)  13.4 us
    dot_general x1, matrix products, shards(): jnp.einsum('erf,efd->erd', hidden, expert_down_w, preferred_element_type=...  9.82 us
  transfers between devices with their start and end apart: 3, of which 3 were waited for; matrix products, arithmetic and copies ran while one was open for 2% of the time, Pallas kernels for 0%

commit v1 on v0

--- a/solution.py
+++ b/solution.py
@@ -146,7 +146,9 @@
     rounded_partial = lax.optimization_barrier(partial_value.astype(jnp.bfloat16)).astype(
         jnp.float32
     )
-    attended = lax.psum(rounded_partial.astype(jnp.bfloat16), "tp").astype(jnp.float32)
+    attended = jnp.sum(lax.all_gather(rounded_partial.astype(jnp.bfloat16), "tp"), axis=0).astype(
+        jnp.float32
+    )
     mixed = residual.astype(jnp.float32) + attended
     normal_rows = rms_scale(mixed, mix_gain).astype(jnp.bfloat16)
     group_count = router_group.shape[1]

time: 231 us -> 220 us (0.952)
  waiting for transfers between devices: 85.8 us -> 73.9 us
    psum x1 -> x0, waiting for transfers between devices: 42.1 us -> none  [shards(): lax.psum(rounded_partial.astype(jnp.bfloat16), 'tp').astype(jnp.float32)]
    all_gather x0 -> x1, waiting for transfers between devices: none -> 30.3 us  [shards(): lax.all_gather(rounded_partial.astype(jnp.bfloat16), 'tp')]
where the time goes in v1:
time: 220 us; the launch traced here: 219 us
  blocking collectives  79.8 us (36%)
  waiting for transfers between devices  73.9 us (34%)
  matrix products  20.9 us (10%)
  local copies, waits for them, and re-layouts  13.9 us (6%)
  between operations  13.8 us (6%)
  other arithmetic  12.4 us (6%)
  starting transfers between devices  4.65 us (2%)
    all_to_all x1, blocking collectives, shards(): lax.all_to_all(outgoing, 'sp', split_axis=0, concat_axis=1, tiled=True)  47.8 us
    all_gather x1, waiting for transfers between devices, shards(): lax.all_gather(rounded_partial.astype(jnp.bfloat16), 'tp')  30.3 us
    reduce_scatter x1, waiting for transfers between devices, shards(): lax.psum_scatter(rounded_down.astype(jnp.bfloat16), 'tp', scatter_dimensi...  30.2 us
    all_gather x1, blocking collectives, shards(): lax.all_gather(normed, 'sp', axis=0, tiled=True)  16.2 us
    all_gather x1, blocking collectives, shards(): key_rot = lax.all_gather(key_turned, 'sp', axis=0, tiled=True)  15.7 us
    all_to_all x1, waiting for transfers between devices, shards(): lax.all_to_all(shaped_out, 'sp', split_axis=2, concat_axis=0, tiled=True)  13.4 us
    dot_general x1, matrix products, shards(): jnp.einsum('erf,efd->erd', hidden, expert_down_w, preferred_element_type=...  9.82 us
    all_to_all x1, starting transfers between devices, shards(): lax.all_to_all(shaped_out, 'sp', split_axis=2, concat_axis=0, tiled=True)  4.61 us
  transfers between devices with their start and end apart: 3, of which 3 were waited for; matrix products, arithmetic and copies ran while one was open for 2% of the time, Pallas kernels for 0%

profile of v1, /device:TPU:0, one launch (start us, length us, event | category | flops | bytes accessed | tf_op | source)
XLA Modules:
  0.0 219.2 jit_solution(10030827468064611122)
XLA Ops:
  6.6 0.9 convert_element_type.98
  7.5 1.1 copy.55
  8.6 1.0 copy.69
  9.6 0.1 multiply_cosine_fusion
  9.8 15.7 %all-gather.1 = bf16[8,112,64]{1,2,0:T(8,128)(2,1)S(1)} all-gather(bf16[1,112,64]{1,2,0:T(8,128)(2,1)S(1)} %maximum_bitcast_fusion), channel_id=1, replica_groups=mesh['sp'=8,'tp'=4] {'sp'}, dimensions={0}, use_global_device_ids=true | all-gather | bytes 129024 | tf_op jit(solution)/shard_map/all_gather | solution.py:129
  25.6 0.1 reshape.333
  25.7 1.0 fusion.36
  26.8 1.0 fusion.38
  27.8 16.2 %all_gather.12 = bf16[896,512]{1,0:T(8,128)(2,1)S(1)} all-gather(bf16[112,512]{1,0:T(8,128)(2,1)S(1)} %fusion.38), channel_id=1, replica_groups=mesh['sp'=8,'tp'=4] {'sp'}, dimensions={0}, use_global_device_ids=true | all-gather | bytes 1032192 | tf_op jit(solution)/shard_map/all_gather | solution.py:123
  44.0 0.8 convolution_convert_fusion
  44.8 0.4 fusion.39
  45.4 0.4 copy-done.4
  45.7 0.5 convolution_convert_fusion.2
  46.2 0.4 fusion.44
  46.7 0.4 fusion.14
  47.1 0.9 select_reduce_fusion
  48.1 0.5 convolution_convert_fusion.3
  48.6 0.8 convolution_convert_fusion.1
  49.3 0.8 fusion.19
  50.2 0.5 fusion.25
  50.7 0.6 fusion.24
  51.3 0.5 fusion.41
  51.8 0.7 copy-done.3
  52.5 1.1 fusion.12
  54.0 0.6 reduce-window.6
  54.6 0.2 slice_reduce_fusion
  55.2 1.3 scatter_custom_fusion.1
  56.5 1.5 scatter_custom_fusion
  58.2 30.3 %all-gather.4.cloned.1.call-done = bf16[448,2048]{1,0:T(8,128)(2,1)} async-done(((bf16[112,2048]{1,0:T(8,128)(2,1)}), bf16[448,2048]{1,0:T(8,128)(2,1)}) %all-gather.4.cloned.1.call-update) | async-done | bytes 1835024 | tf_op jit(solution)/shard_map/all_gather | solution.py:149
  88.5 1.9 reduce_sum.107
  90.3 1.2 convert_add_fusion
  91.6 0.2 multiply_convert_fusion.1
  91.8 3.2 %gather_fusion = bf16[448,2048]{1,0:T(8,128)(2,1)} fusion(bf16[112,2048]{1,0:T(8,128)(2,1)S(1)} %multiply_convert_fusion.1, s32[1024]{0:T(1024)S(1)} %pad_clamp_fusion.1), kind=kCustom, calls=%fused_computation | custom fusion | bytes 3671808 | tf_op jit(solution)/shard_map/gather | solution.py:179
  95.0 1.8 broadcast_select_fusion
  96.8 47.8 %all_to_all.8 = bf16[8,56,2048]{2,1,0:T(8,128)(2,1)S(1)} all-to-all(bf16[8,56,2048]{2,1,0:T(8,128)(2,1)S(1)} %broadcast_select_fusion), channel_id=1, replica_groups=mesh['sp'=8,'tp'=4] {'sp'}, dimensions={0} | all-to-all | bytes 3670016 | tf_op jit(solution)/shard_map/all_to_all | solution.py:181
  144.7 1.3 copy-done.1
  145.9 3.3 %fusion.4 = f32[448,1024]{1,0:T(8,128)} fusion(bf16[448,2048]{1,0:T(8,128)(2,1)S(1)} %bitcast.100, bf16[1,2048,1024]{2,1,0:T(8,128)(2,1)S(1)} %copy-done.10), kind=kOutput, calls=%fused_computation.8 | convolution fusion | flops 1879048192 | bytes 7864320 | tf_op jit(solution)/shard_map/erd,edf->erf/dot_general | solution.py:183
  149.3 9.8 %fusion.9 = bf16[1,448,2048]{2,1,0:T(8,128)(2,1)} fusion(bf16[1,1024,2048]{2,1,0:T(8,128)(2,1)} %param.37, f32[448,1024]{1,0:T(8,128)} %fusion.4, bf16[448,2048]{1,0:T(8,128)(2,1)} %bitcast.101, bf16[1,2048,1024]{2,1,0:T(8,128)(2,1)} %param.36), kind=kOutput, calls=%fused_computation.11 | convolution fusion | flops 3761766400 | bytes 13893632 | tf_op jit(solution)/shard_map/erf,efd->erd/dot_general | solution.py:190
  159.2 0.7 copy-done.6
  159.8 0.2 fusion.69
  160.1 30.2 %reduce-scatter.2.cloned.1.call-done = bf16[1,448,512]{2,1,0:T(8,128)(2,1)} async-done(((bf16[1,448,2048]{2,1,0:T(8,128)(2,1)}), bf16[1,448,512]{2,1,0:T(8,128)(2,1)}) %reduce-scatter.2.cloned.1.call-update) | async-done | bytes 458768 | tf_op jit(solution)/shard_map/reduce_scatter | solution.py:194
  190.2 4.6 %all-to-all-start.1 = ((bf16[1,1,8,56,512]{4,3,1,0,2:T(8,128)(2,1)}), bf16[1,1,8,56,512]{4,3,1,0,2:T(8,128)(2,1)S(1)}, u32[]{:S(2)}, u32[]{:S(2)}) async-start(bf16[1,1,8,56,512]{4,3,1,0,2:T(8,128)(2,1)} %bitcast.108), calls=%async_computation.2 | async-start | bytes 917504 | tf_op jit(solution)/shard_map/all_to_all | solution.py:199
  194.9 0.2 fusion.68
  195.4 13.4 %all-to-all-done.1 = bf16[1,1,8,56,512]{4,3,1,0,2:T(8,128)(2,1)S(1)} async-done(((bf16[1,1,8,56,512]{4,3,1,0,2:T(8,128)(2,1)}), bf16[1,1,8,56,512]{4,3,1,0,2:T(8,128)(2,1)S(1)}, u32[]{:S(2)}, u32[]{:S(2)}) %all-to-all-start.1) | async-done | bytes 458784 | tf_op jit(solution)/shard_map/all_to_all | solution.py:199
  208.8 1.1 gather_fusion.1
  209.9 0.3 reshape.296
  210.2 0.6 multiply_reduce_fusion.1
  210.8 1.6 add_convert_fusion
  (64 shorter events, 1.5 us)
Async XLA Ops:
  6.5 44.8 %copy-start = (bf16[512,2048]{1,0:T(8,128)(2,1)S(1)}, bf16[512,2048]{1,0:T(8,128)(2,1)}, u32[]{:S(2)}) copy-start(bf16[512,2048]{1,0:T(8,128)(2,1)} %param.29) | copy-start | bytes 6291460
  6.5 37.5 %copy-start.11 = (bf16[512,512]{1,0:T(8,128)(2,1)S(1)}, bf16[512,512]{1,0:T(8,128)(2,1)}, u32[]{:S(2)}) copy-start(bf16[512,512]{1,0:T(8,128)(2,1)} %param.25) | copy-start | bytes 1572868
  6.5 81.9 %all-gather.4.cloned.1.call-start = ((), (), s32[]{:S(2)}) async-start(), calls=%async_computation.4 | async-start | bytes 2293760 | tf_op jit(solution)/shard_map/all_gather | solution.py:149
  44.8 1.0 copy-start.4
  47.1 1.0 copy-start.5
  47.1 1.4 copy-start.12
  51.3 1.2 copy-start.3
  51.8 1.9 copy-start.8
  53.6 36.7 %copy-start.2 = (bf16[112,2048]{1,0:T(8,128)(2,1)S(1)}, bf16[112,2048]{1,0:T(8,128)(2,1)}, u32[]{:S(2)}) copy-start(bf16[112,2048]{1,0:T(8,128)(2,1)} %param.19) | copy-start | bytes 1376260
  53.7 136.6 %reduce-scatter.2.cloned.1.call-start = ((), (), s32[]{:S(2)}) async-start(), calls=%async_computation.3 | async-start | bytes 2293760 | tf_op jit(solution)/shard_map/reduce_scatter | solution.py:194
  88.5 3.1 %copy-start.9 = (f32[2048]{0:T(1024)S(1)}, f32[2048]{0:T(1024)}, u32[]{:S(2)}) copy-start(f32[2048]{0:T(1024)} %param.31) | copy-start | bytes 24580
  95.0 50.9 %copy-start.10 = (bf16[1,2048,1024]{2,1,0:T(8,128)(2,1)S(1)}, bf16[1,2048,1024]{2,1,0:T(8,128)(2,1)}, u32[]{:S(2)}) copy-start(bf16[1,2048,1024]{2,1,0:T(8,128)(2,1)} %param.35) | copy-start | bytes 12582916
  144.7 1.3 copy-start.1
  159.1 0.8 copy-start.6
  159.1 35.8 %copy-start.7 = (bf16[2048,4]{0,1:T(4,128)(2,1)S(1)}, bf16[2048,4]{0,1:T(4,128)(2,1)}, u32[]{:S(2)}) copy-start(bf16[2048,4]{0,1:T(4,128)(2,1)} %param.32) | copy-start | bytes 49156
  190.2 18.5 %all-to-all-start.1 = ((bf16[1,1,8,56,512]{4,3,1,0,2:T(8,128)(2,1)}), bf16[1,1,8,56,512]{4,3,1,0,2:T(8,128)(2,1)S(1)}, u32[]{:S(2)}, u32[]{:S(2)}) async-start(bf16[1,1,8,56,512]{4,3,1,0,2:T(8,128)(2,1)} %bitcast.108), calls=%async_computation.2 | async-start | bytes 917504 | tf_op jit(solution)/shard_map/all_to_all | solution.py:199
Sparse Core Ops, SparseCore 0:
  53.8 34.6 all-gather.3
  159.2 30.9 reduce-scatter.1
